TPU v7x, 32 devices: a whole 2x2x4 slice. The times are simulated.
32 devices in a mesh: gr: 2 (over y), sp: 4 (over z), tp: 4 (over x, core).
Axes of the slice: x: 2, y: 2, z: 4, core: 2. Of those that a mesh axis runs over, the one named last changes fastest.
Arguments:
- tokens: bfloat16 [8, 8192, 2048], P(('gr', 'tp'), 'sp'), may hold values from -6 to 6
- kv_weight: bfloat16 [2048, 1024], replicated, may hold values from -0.125 to 0.125
- queries: bfloat16 [8, 1536], P(('gr', 'tp')), may hold values from -6 to 6
- score_offset: float32 [24], replicated, may hold values from -10.5 to -3.5
Outputs:
- cache: bfloat16 [8, 4, 8192, 256], P(('gr', 'tp'), 'sp')
- read: bfloat16 [8, 1536], P(('gr', 'tp'))
All inputs are finite; a program needn't handle non-finite values.
Results may differ from a plain program's by a relative error of at most 0.0085.
Values may be sent and summed in bfloat16 or wider, within the bound.
A program may use at most 64 MiB of HBM per device.

v0:
```python
import functools

import jax
import jax.numpy as jnp
from jax import lax
from jax.experimental import pallas as pl
from jax.experimental.pallas import tpu as pltpu
from jax.sharding import PartitionSpec as P

KVH = 8
HD = 64


def prefix(shard, axis, combine, identity):
    size, index = (lax.axis_size(axis), lax.axis_index(axis))
    everything = lax.all_gather(shard, axis)
    start = jnp.broadcast_to(jnp.asarray(identity, shard.dtype), shard.shape)

    def hop(k, before):
        at = size - 1 - k
        reached = at > index
        new = combine(before, everything[at])
        return jnp.where(reached, new, before)

    return lax.fori_loop(0, size, hop, start)


def add_terms(earlier, later):
    return earlier + later


def finish(contribution):
    return lax.psum(contribution, "sp").astype(jnp.bfloat16)


def local_plain(tokens, kv_weight, queries, score_offset):
    seq_count, pos_rows, model_width = tokens.shape
    features = kv_weight.shape[1]
    slot_count = lax.axis_size("sp")
    blocks = slot_count // seq_count
    block_width = features // blocks
    half_blocks = blocks // 2
    heads = score_offset.shape[0]
    group_size = heads // KVH
    per_block = block_width // HD
    projected = jnp.einsum(
        "spd,dcw->scpw",
        tokens,
        kv_weight.reshape(model_width, blocks, block_width),
        preferred_element_type=jnp.float32,
    ).astype(jnp.bfloat16)
    received = lax.all_to_all(
        projected.reshape(slot_count, pos_rows, block_width),
        "sp",
        split_axis=0,
        concat_axis=1,
        tiled=True,
    )
    length = received.shape[1]
    cache = received.reshape(1, 1, length, block_width)
    key_part = projected[:, :half_blocks].reshape(seq_count, half_blocks, pos_rows, per_block, HD)
    value_part = (
        projected[:, half_blocks:]
        .reshape(seq_count, half_blocks, pos_rows, per_block, HD)
        .astype(jnp.float32)
    )
    query_heads = queries.reshape(seq_count, half_blocks, per_block, group_size, HD)
    offsets = score_offset.reshape(half_blocks, per_block, group_size)
    logits = jnp.einsum(
        "scvgd,scpvd->scvgp", query_heads, key_part, preferred_element_type=jnp.float32
    )
    logits = logits * HD ** (-0.5) + offsets[None, :, :, :, None]
    keep_log = jax.nn.log_sigmoid(-logits)
    between = lax.cumsum(keep_log, axis=4, reverse=True) - keep_log
    totals = jnp.sum(keep_log, axis=4)
    later_keep = prefix(totals, "sp", add_terms, jnp.zeros_like(totals))
    weights = jnp.exp(jax.nn.log_sigmoid(logits) + between + later_keep[..., None])
    weighted = jnp.einsum("scvgp,scpvd->scvgd", weights, value_part)
    contribution = weighted.reshape(seq_count, heads * HD)
    return (cache, finish(contribution))


CHUNK = 128
VMEM_LIMIT = 56 * 2**20
LANES = 128
MESH = pl.DeviceIdType.MESH


def exchange_kernel(
    count,
    tok_hbm,
    w_hbm,
    q_ref,
    off_ref,
    recv,
    read_ref,
    tok,
    wts,
    proj,
    qbig,
    part,
    parts,
    tok_sem,
    w_sem,
    send_sem,
    recv_sem,
    psend_sem,
    precv_sem,
):
    me = lax.axis_index("sp")
    rows = tok.shape[0]
    width = wts.shape[2]
    chunks = rows // CHUNK
    heads = off_ref.shape[1]
    group = heads // KVH
    half = count // 2

    lower = me < count // 2

    def dest(j):
        if j == count - 1:
            return me
        down = count - 1 - j
        return jnp.where(
            lower,
            jnp.where(down > me, down, down - 1),
            jnp.where(j < me, j, j + 1),
        )

    def tok_copy(c):
        at = pl.ds(pl.multiple_of(c * CHUNK, CHUNK), CHUNK)
        return pltpu.make_async_copy(tok_hbm.at[at, :], tok.at[at, :], tok_sem.at[c])

    def w_copy(d):
        at = pl.ds(pl.multiple_of(d * width, width), width)
        return pltpu.make_async_copy(w_hbm.at[:, at], wts.at[d], w_sem.at[d])

    barrier = pltpu.get_barrier_semaphore()
    for j in range(count - 1):
        pl.semaphore_signal(barrier, inc=1, device_id={"sp": dest(j)}, device_id_type=MESH)

    tok_copy(chunks - 1).start()
    for j in range(2):
        w_copy(dest(j)).start()

    q_rows = []
    for h in range(heads):
        pair = q_ref[:, h // 2 * LANES : (h // 2 + 1) * LANES].astype(jnp.float32)
        q_rows.append(pair if h % 2 == h // group % 2 else pltpu.roll(pair, HD, axis=1))
    spread = jnp.concatenate(
        [jnp.concatenate(q_rows, axis=0)] * (KVH * HD // LANES), axis=1
    )
    square = (heads, heads)
    diagonal = lax.broadcasted_iota(jnp.int32, square, 0) == lax.broadcasted_iota(
        jnp.int32, square, 1
    )
    offsets = jnp.sum(
        jnp.where(diagonal, jnp.broadcast_to(off_ref[...], square), 0.0), axis=1, keepdims=True
    )
    column = lax.broadcasted_iota(jnp.int32, spread.shape, 1) // HD
    row = lax.broadcasted_iota(jnp.int32, spread.shape, 0) // group
    mine = column == row
    qbig[...] = jnp.where(mine, spread, 0.0).astype(jnp.bfloat16)
    earlier = lax.broadcasted_iota(jnp.int32, (CHUNK, CHUNK), 1)
    later = lax.broadcasted_iota(jnp.int32, (CHUNK, CHUNK), 0)
    after = jnp.where(later > earlier, 1.0, 0.0).astype(jnp.bfloat16)

    def deferred(d):
        inner = jnp.logical_and(d > 0, d < count - 1)
        return jnp.logical_and(inner, (d < count // 2) != (me < count // 2))

    def block_copy(d, c):
        here = pl.ds(pl.multiple_of(c * CHUNK, CHUNK), CHUNK)
        there = pl.ds(pl.multiple_of(me * rows + c * CHUNK, CHUNK), CHUNK)
        return pltpu.make_async_remote_copy(
            src_ref=proj.at[d, here, :],
            dst_ref=recv.at[there, :],
            send_sem=send_sem.at[d],
            recv_sem=recv_sem.at[me],
            device_id={"sp": d},
            device_id_type=MESH,
        )

    def step(i, state):
        kept, total = state
        c = chunks - 1 - i
        at = pl.ds(pl.multiple_of(c * CHUNK, CHUNK), CHUNK)
        tok_copy(c).wait()
        for j in range(count):
            d = dest(j)

            @pl.when(i == 0)
            def _():
                w_copy(d).wait()
                if j == 0:
                    for k in range(2, count):
                        w_copy(dest(k)).start()
                    tok_copy(c - 1).start()

            if j == 0:

                @pl.when(i + 2 < chunks)
                def _():
                    tok_copy(c - 2).start()

            block = jnp.dot(
                tok[at, :], wts[d], preferred_element_type=jnp.float32
            ).astype(jnp.bfloat16)
            proj[d, at, :] = block
            if j == count - 1:
                own = pl.ds(pl.multiple_of(me * rows + c * CHUNK, CHUNK), CHUNK)
                recv[own, :] = block
            if j > 0:
                before = dest(j - 1)
                if j == 1:

                    @pl.when(i == 0)
                    def _():
                        pl.semaphore_wait(barrier, count - 1)

                @pl.when(jnp.logical_not(deferred(before)))
                def _():
                    block_copy(before, c).start()

        logits = jnp.zeros((heads, CHUNK), jnp.float32)
        for b in range(half):
            logits = logits + lax.dot_general(
                qbig[:, b * width : (b + 1) * width],
                proj[b, at, :],
                (((1,), (1,)), ((), ())),
                preferred_element_type=jnp.float32,
            )
        logits = logits * HD ** (-0.5) + offsets
        keep = -(jnp.maximum(logits, 0.0) + jnp.log1p(jnp.exp(-jnp.abs(logits))))
        high = keep.astype(jnp.bfloat16)
        rest = keep - high.astype(jnp.float32)
        mid = rest.astype(jnp.bfloat16)
        low = (rest - mid.astype(jnp.float32)).astype(jnp.bfloat16)
        sums = jnp.dot(
            jnp.concatenate([high, mid, low], axis=0), after, preferred_element_type=jnp.float32
        )
        between = sums[:heads] + sums[heads : 2 * heads] + sums[2 * heads :]
        weight = jnp.exp(logits + keep + between + kept)
        weight_high = weight.astype(jnp.bfloat16)
        weight_low = (weight - weight_high.astype(jnp.float32)).astype(jnp.bfloat16)
        both = jnp.concatenate([weight_high, weight_low], axis=0)
        summed = jnp.concatenate(
            [
                jnp.dot(both, proj[half + b, at, :], preferred_element_type=jnp.float32)
                for b in range(half)
            ],
            axis=1,
        )
        total = total + summed[:heads] + summed[heads:]
        kept = kept + jnp.sum(keep, axis=1, keepdims=True)
        return kept, total

    kept, total = lax.fori_loop(
        0,
        chunks,
        step,
        (jnp.zeros((heads, 1), jnp.float32), jnp.zeros((heads, KVH * HD), jnp.float32)),
    )
    total = jnp.where(mine, total, 0.0)
    folded = total[:, :LANES]
    for g in range(1, KVH * HD // LANES):
        folded = folded + total[:, g * LANES : (g + 1) * LANES]
    spread_kept = jnp.broadcast_to(kept, (heads, LANES))
    part[0] = folded
    part[1] = spread_kept
    parts[me, 0] = folded
    parts[me, 1] = spread_kept

    @pl.loop(0, 1)
    def _(i):
        for j in range(count - 1):
            d = dest(j)

            @pl.when(deferred(d))
            def _():
                block_copy(d, chunks - 1 - i).start()

    def part_copy(d):
        return pltpu.make_async_remote_copy(
            src_ref=part,
            dst_ref=parts.at[me],
            send_sem=psend_sem.at[d],
            recv_sem=precv_sem.at[me],
            device_id={"sp": d},
            device_id_type=MESH,
        )

    for j in range(count - 1):
        part_copy(dest(j)).start()

    @pl.loop(1, chunks)
    def _(i):
        for j in range(count - 1):
            d = dest(j)

            @pl.when(deferred(d))
            def _():
                block_copy(d, chunks - 1 - i).start()

    for j in range(count - 1):
        d = dest(j)
        pltpu.make_async_remote_copy(
            src_ref=part,
            dst_ref=parts.at[d],
            send_sem=psend_sem.at[d],
            recv_sem=precv_sem.at[d],
            device_id={"sp": d},
            device_id_type=MESH,
        ).wait()
    left = jnp.zeros((heads, LANES), jnp.float32)
    out = jnp.zeros((heads, LANES), jnp.float32)
    for z in range(count - 1, -1, -1):
        out = out + jnp.exp(left) * parts[z, 0]
        left = left + parts[z, 1]
    turned = pltpu.roll(out, HD, axis=1)
    low_half = lax.broadcasted_iota(jnp.int32, (1, LANES), 1) < HD
    for m in range(heads // 2):
        first, second = 2 * m, 2 * m + 1
        from_first = out if (first // group) % 2 == 0 else turned
        from_second = out if (second // group) % 2 == 1 else turned
        piece = jnp.where(
            low_half, from_first[first : first + 1], from_second[second : second + 1]
        )
        read_ref[:, m * LANES : (m + 1) * LANES] = piece.astype(read_ref.dtype)
    for j in range(count - 1):
        d = dest(j)
        pltpu.make_async_remote_copy(
            src_ref=proj.at[d],
            dst_ref=recv.at[pl.ds(pl.multiple_of(d * rows, CHUNK), rows), :],
            send_sem=send_sem.at[d],
            recv_sem=recv_sem.at[d],
            device_id={"sp": d},
            device_id_type=MESH,
        ).wait()


def place_kernel(count, got, read, cache, read_out, sems):
    rows = got.shape[0] // count
    copies = []
    for k in range(count):
        at = pl.ds(k * rows, rows)
        copies.append(pltpu.make_async_copy(got.at[at, :], cache.at[at, :], sems.at[k]))
    copies.append(pltpu.make_async_copy(read, read_out, sems.at[count]))
    for copy in copies:
        copy.start()
    for copy in copies:
        copy.wait()


def local(tokens, kv_weight, queries, score_offset):
    seq_count, rows, model_width = tokens.shape
    features = kv_weight.shape[1]
    heads = score_offset.shape[0]
    count = lax.axis_size("sp")
    width = features // (count // seq_count)
    fits = (
        seq_count == 1
        and count % 2 == 0
        and count > 2
        and width % LANES == 0
        and rows % CHUNK == 0
        and rows >= 2 * CHUNK
        and features == 2 * KVH * HD
        and 2 * HD == LANES
        and heads % 2 == 0
    )
    if not fits:
        return local_plain(tokens, kv_weight, queries, score_offset)
    length = rows * count
    vmem = pl.BlockSpec(memory_space=pltpu.VMEM)
    hbm = pl.BlockSpec(memory_space=pltpu.HBM)
    got, read = pl.pallas_call(
        functools.partial(exchange_kernel, count),
        out_shape=(
            pltpu.VMEM((length, width), jnp.bfloat16),
            pltpu.VMEM((1, heads * HD), jnp.bfloat16),
        ),
        in_specs=[hbm, hbm, vmem, vmem],
        out_specs=(vmem, vmem),
        scratch_shapes=[
            pltpu.VMEM((rows, model_width), jnp.bfloat16),
            pltpu.VMEM((count, model_width, width), jnp.bfloat16),
            pltpu.VMEM((count, rows, width), jnp.bfloat16),
            pltpu.VMEM((heads, KVH * HD), jnp.bfloat16),
            pltpu.VMEM((2, heads, LANES), jnp.float32),
            pltpu.VMEM((count, 2, heads, LANES), jnp.float32),
            pltpu.SemaphoreType.DMA((rows // CHUNK,)),
            pltpu.SemaphoreType.DMA((count,)),
            pltpu.SemaphoreType.DMA((count,)),
            pltpu.SemaphoreType.DMA((count,)),
            pltpu.SemaphoreType.DMA((count,)),
            pltpu.SemaphoreType.DMA((count,)),
        ],
        compiler_params=pltpu.CompilerParams(
            collective_id=0, has_side_effects=True, vmem_limit_bytes=VMEM_LIMIT
        ),
    )(
        tokens.reshape(rows, model_width),
        kv_weight,
        queries,
        score_offset.reshape(1, heads),
    )
    cache, read = pl.pallas_call(
        functools.partial(place_kernel, count),
        out_shape=(
            jax.ShapeDtypeStruct((length, width), jnp.bfloat16),
            jax.ShapeDtypeStruct((1, heads * HD), jnp.bfloat16),
        ),
        in_specs=[vmem, vmem],
        out_specs=(hbm, hbm),
        scratch_shapes=[pltpu.SemaphoreType.DMA((count + 1,))],
        compiler_params=pltpu.CompilerParams(vmem_limit_bytes=8 * 2**20),
    )(got, read)
    return cache.reshape(1, 1, length, width), read


def solution(mesh):
    placed = (P(("gr", "tp"), "sp", None), P(), P(("gr", "tp"), None), P())
    return jax.shard_map(
        local,
        mesh=mesh,
        in_specs=placed,
        out_specs=(P(("gr", "tp"), "sp", None, None), P(("gr", "tp"), None)),
        check_vma=False,
    )
```

profile of v0, /device:TPU:9, one launch (start us, length us, event | category | flops | bytes accessed | tf_op | source)
XLA Modules:
  0.0 100.3 jit_solution(9034076158002239927)
XLA Ops:
  0.6 97.7 %shard_map.59 = (bf16[8192,256]{1,0:T(8,128)(2,1)S(1)}, bf16[1,1536]{1,0:T(2,128)(2,1)S(1)}) custom-call(bf16[2048,2048]{1,0:T(8,128)(2,1)} %bitcast.3, bf16[2048,1024]{1,0:T(8,128)(2,1)} %w_hbm.1, bf16[1,1536]{1,0:T(2,128)(2,1)} %q_ref.1, f32[1,24]{1,0:T(1,128)} %bitcast.4), custom_call_target="tpu_custom_call" | custom-call | tf_op jit(solution)/shard_map/pallas_call | solution.py:377
  98.3 2.1 %shard_map.60 = (bf16[8192,256]{1,0:T(8,128)(2,1)}, bf16[1,1536]{1,0:T(2,128)(2,1)}) custom-call(bf16[8192,256]{1,0:T(8,128)(2,1)S(1)} %get-tuple-element.6.got, bf16[1,1536]{1,0:T(2,128)(2,1)S(1)} %get-tuple-element.7.read), custom_call_target="tpu_custom_call" | custom-call | tf_op jit(solution)/shard_map/pallas_call | solution.py:408
where the time goes:
time: 101 us; the launch traced here: 100 us
  Pallas kernels  99.7 us (99%)
    pallas_call x1, Pallas kernels, local(): pl.pallas_call(functools.partial(exchange_kernel, count), out_shape=(pltp...  97.7 us
    pallas_call x1, Pallas kernels, local(): pl.pallas_call(functools.partial(place_kernel, count), out_shape=(jax.Sha...  2.05 us

commit v1 on v0

--- a/solution.py
+++ b/solution.py
@@ -81,6 +81,9 @@
 
 
 CHUNK = 128
+EARLY = 4
+SLICES = 4
+PLACES = 4
 VMEM_LIMIT = 56 * 2**20
 LANES = 128
 MESH = pl.DeviceIdType.MESH
@@ -99,23 +102,37 @@
     proj,
     qbig,
     part,
-    parts,
+    whole,
+    outer_part,
+    other_part,
+    inner_whole,
     tok_sem,
     w_sem,
+    slice_sem,
     send_sem,
     recv_sem,
     psend_sem,
     precv_sem,
+    ready,
+    everyone,
 ):
     me = lax.axis_index("sp")
     rows = tok.shape[0]
+    model_width = tok.shape[1]
     width = wts.shape[2]
     chunks = rows // CHUNK
     heads = off_ref.shape[1]
     group = heads // KVH
     half = count // 2
-
-    lower = me < count // 2
+    depth = model_width // SLICES
+
+    lower = me < half
+    inner = jnp.where(lower, half - 1, half)
+    mate = jnp.where(lower, half, half - 1)
+    is_inner = me == inner
+    inward = jnp.where(lower, me + 1, me - 1)
+    outward = jnp.where(lower, me - 1, me + 1)
+    has_outer = jnp.logical_and(me > 0, me < count - 1)
 
     def dest(j):
         if j == count - 1:
@@ -127,21 +144,90 @@
             jnp.where(j < me, j, j + 1),
         )
 
+    def span(c):
+        return pl.ds(pl.multiple_of(c * CHUNK, CHUNK), CHUNK)
+
     def tok_copy(c):
-        at = pl.ds(pl.multiple_of(c * CHUNK, CHUNK), CHUNK)
-        return pltpu.make_async_copy(tok_hbm.at[at, :], tok.at[at, :], tok_sem.at[c])
+        return pltpu.make_async_copy(tok_hbm.at[span(c), :], tok.at[span(c), :], tok_sem.at[c])
 
     def w_copy(d):
         at = pl.ds(pl.multiple_of(d * width, width), width)
         return pltpu.make_async_copy(w_hbm.at[:, at], wts.at[d], w_sem.at[d])
 
+    def slice_copy(k):
+        at = pl.ds(pl.multiple_of(mate * width, width), width)
+        deep = pl.ds(k * depth, depth)
+        return pltpu.make_async_copy(
+            w_hbm.at[deep, at], wts.at[mate, deep, :], slice_sem.at[k]
+        )
+
+    def block_copy(d, c):
+        there = pl.ds(pl.multiple_of(me * rows + c * CHUNK, CHUNK), CHUNK)
+        return pltpu.make_async_remote_copy(
+            src_ref=proj.at[d, span(c), :],
+            dst_ref=recv.at[there, :],
+            send_sem=send_sem.at[d],
+            recv_sem=recv_sem.at[me],
+            device_id={"sp": d},
+            device_id_type=MESH,
+        )
+
     barrier = pltpu.get_barrier_semaphore()
-    for j in range(count - 1):
-        pl.semaphore_signal(barrier, inc=1, device_id={"sp": dest(j)}, device_id_type=MESH)
+
+    @pl.when(is_inner)
+    def _():
+        pl.semaphore_signal(barrier, inc=1, device_id={"sp": mate}, device_id_type=MESH)
 
     tok_copy(chunks - 1).start()
-    for j in range(2):
-        w_copy(dest(j)).start()
+    for k in range(SLICES):
+        slice_copy(k).start()
+
+    first = jnp.zeros((CHUNK, width), jnp.float32)
+    tok_copy(chunks - 1).wait()
+    for k in range(SLICES):
+        slice_copy(k).wait()
+        if k == 0:
+            tok_copy(chunks - 2).start()
+            w_copy(dest(0)).start()
+        deep = pl.ds(k * depth, depth)
+        first = first + jnp.dot(
+            tok[span(chunks - 1), deep], wts[mate, deep, :], preferred_element_type=jnp.float32
+        )
+    proj[mate, span(chunks - 1), :] = first.astype(jnp.bfloat16)
+    for k in range(2, EARLY):
+        tok_copy(chunks - 1 - k).start()
+    for j in range(1, count):
+        if j != half - 1:
+            w_copy(dest(j)).start()
+    pl.semaphore_wait(barrier, 1)
+    block_copy(mate, chunks - 1).start()
+
+    for d in range(count):
+        same = (d < half) == lower
+
+        @pl.when(jnp.logical_and(is_inner, jnp.logical_and(same, d != me)))
+        def _():
+            pl.semaphore_signal(barrier, inc=1, device_id={"sp": d}, device_id_type=MESH)
+
+    @pl.when(jnp.logical_not(is_inner))
+    def _():
+        for d in (half - 1, half):
+            pl.semaphore_signal(ready, inc=1, device_id={"sp": d}, device_id_type=MESH)
+
+    def early(k, carry):
+        c = chunks - 1 - k
+        tok_copy(c).wait()
+        proj[mate, span(c), :] = jnp.dot(
+            tok[span(c), :], wts[mate], preferred_element_type=jnp.float32
+        ).astype(jnp.bfloat16)
+
+        @pl.when(k > 1)
+        def _():
+            block_copy(mate, c + 1).start()
+
+        return carry
+
+    lax.fori_loop(1, EARLY, early, 0)
 
     q_rows = []
     for h in range(heads):
@@ -150,12 +236,29 @@
     spread = jnp.concatenate(
         [jnp.concatenate(q_rows, axis=0)] * (KVH * HD // LANES), axis=1
     )
+    diagonal = lax.broadcasted_iota(jnp.int32, (heads, LANES), 0) == lax.broadcasted_iota(
+        jnp.int32, (heads, LANES), 1
+    )
+
+    def to_column(row):
+        return jnp.sum(
+            jnp.where(diagonal, jnp.broadcast_to(row, (heads, LANES)), 0.0), axis=1, keepdims=True
+        )
+
+    def to_row(column):
+        return jnp.sum(
+            jnp.where(diagonal, jnp.broadcast_to(column, (heads, LANES)), 0.0),
+            axis=0,
+            keepdims=True,
+        )
+
     square = (heads, heads)
-    diagonal = lax.broadcasted_iota(jnp.int32, square, 0) == lax.broadcasted_iota(
-        jnp.int32, square, 1
-    )
     offsets = jnp.sum(
-        jnp.where(diagonal, jnp.broadcast_to(off_ref[...], square), 0.0), axis=1, keepdims=True
+        jnp.where(
+            diagonal[:, :heads], jnp.broadcast_to(off_ref[...], square), 0.0
+        ),
+        axis=1,
+        keepdims=True,
     )
     column = lax.broadcasted_iota(jnp.int32, spread.shape, 1) // HD
     row = lax.broadcasted_iota(jnp.int32, spread.shape, 0) // group
@@ -165,62 +268,74 @@
     later = lax.broadcasted_iota(jnp.int32, (CHUNK, CHUNK), 0)
     after = jnp.where(later > earlier, 1.0, 0.0).astype(jnp.bfloat16)
 
+    block_copy(mate, chunks - EARLY).start()
+
+    @pl.when(is_inner)
+    def _():
+        pl.semaphore_wait(ready, count - 2)
+
+    for d in range(count):
+        same = (d < half) == lower
+
+        @pl.when(jnp.logical_and(is_inner, jnp.logical_and(same, d != me)))
+        def _():
+            pl.semaphore_signal(everyone, inc=1, device_id={"sp": d}, device_id_type=MESH)
+
+    @pl.when(jnp.logical_not(is_inner))
+    def _():
+        pl.semaphore_wait(everyone, 1)
+
     def deferred(d):
-        inner = jnp.logical_and(d > 0, d < count - 1)
-        return jnp.logical_and(inner, (d < count // 2) != (me < count // 2))
-
-    def block_copy(d, c):
-        here = pl.ds(pl.multiple_of(c * CHUNK, CHUNK), CHUNK)
-        there = pl.ds(pl.multiple_of(me * rows + c * CHUNK, CHUNK), CHUNK)
-        return pltpu.make_async_remote_copy(
-            src_ref=proj.at[d, here, :],
-            dst_ref=recv.at[there, :],
-            send_sem=send_sem.at[d],
-            recv_sem=recv_sem.at[me],
-            device_id={"sp": d},
-            device_id_type=MESH,
+        crosses = (d < half) != lower
+        return jnp.logical_or(
+            d == mate, jnp.logical_and(jnp.logical_not(crosses), jnp.logical_not(has_outer))
         )
 
     def step(i, state):
         kept, total = state
         c = chunks - 1 - i
-        at = pl.ds(pl.multiple_of(c * CHUNK, CHUNK), CHUNK)
-        tok_copy(c).wait()
+        at = span(c)
+
+        @pl.when(i >= EARLY)
+        def _():
+            tok_copy(c).wait()
+
+        @pl.when(i + EARLY < chunks)
+        def _():
+            tok_copy(c - EARLY).start()
+
+        before = None
         for j in range(count):
             d = dest(j)
-
-            @pl.when(i == 0)
-            def _():
-                w_copy(d).wait()
-                if j == 0:
-                    for k in range(2, count):
-                        w_copy(dest(k)).start()
-                    tok_copy(c - 1).start()
-
-            if j == 0:
-
-                @pl.when(i + 2 < chunks)
+            if j == half - 1:
+
+                @pl.when(i >= EARLY)
                 def _():
-                    tok_copy(c - 2).start()
-
-            block = jnp.dot(
-                tok[at, :], wts[d], preferred_element_type=jnp.float32
-            ).astype(jnp.bfloat16)
-            proj[d, at, :] = block
-            if j == count - 1:
-                own = pl.ds(pl.multiple_of(me * rows + c * CHUNK, CHUNK), CHUNK)
-                recv[own, :] = block
-            if j > 0:
-                before = dest(j - 1)
-                if j == 1:
-
-                    @pl.when(i == 0)
-                    def _():
-                        pl.semaphore_wait(barrier, count - 1)
-
-                @pl.when(jnp.logical_not(deferred(before)))
+                    proj[mate, at, :] = jnp.dot(
+                        tok[at, :], wts[mate], preferred_element_type=jnp.float32
+                    ).astype(jnp.bfloat16)
+
+            else:
+
+                @pl.when(i == 0)
                 def _():
-                    block_copy(before, c).start()
+                    w_copy(d).wait()
+
+                block = jnp.dot(
+                    tok[at, :], wts[d], preferred_element_type=jnp.float32
+                ).astype(jnp.bfloat16)
+                proj[d, at, :] = block
+                if j == count - 1:
+                    own = pl.ds(pl.multiple_of(me * rows + c * CHUNK, CHUNK), CHUNK)
+                    recv[own, :] = block
+            if before is not None:
+                send = before
+
+                @pl.when(jnp.logical_not(deferred(send)))
+                def _():
+                    block_copy(send, c).start()
+
+            before = None if j == half - 1 else d
 
         logits = jnp.zeros((heads, CHUNK), jnp.float32)
         for b in range(half):
@@ -261,91 +376,151 @@
         step,
         (jnp.zeros((heads, 1), jnp.float32), jnp.zeros((heads, KVH * HD), jnp.float32)),
     )
+
+    pairs = heads // 2
+    left_lanes = lax.broadcasted_iota(jnp.int32, (heads, LANES), 1) < HD
+    left_head = lax.broadcasted_iota(jnp.int32, (heads, LANES), 0) // group % 2 == 0
+
+    def pack(x):
+        x = jnp.where(left_lanes == left_head, x, 0.0)
+        return jnp.concatenate(
+            [
+                x[2 * g * group : (2 * g + 1) * group] + x[(2 * g + 1) * group : (2 * g + 2) * group]
+                for g in range(KVH // 2)
+            ],
+            axis=0,
+        )
+
+    def join(early_sums, early_row, late_sums, late_row):
+        spread_keep = jnp.broadcast_to(to_column(late_row), (heads, LANES))
+        return late_sums + jnp.exp(pack(spread_keep)) * early_sums, early_row + late_row
+
+    def join_sides(sums, row, other_sums, other_row, own_late):
+        return join(
+            jnp.where(own_late, other_sums, sums),
+            jnp.where(own_late, other_row, row),
+            jnp.where(own_late, sums, other_sums),
+            jnp.where(own_late, row, other_row),
+        )
+
     total = jnp.where(mine, total, 0.0)
     folded = total[:, :LANES]
     for g in range(1, KVH * HD // LANES):
         folded = folded + total[:, g * LANES : (g + 1) * LANES]
-    spread_kept = jnp.broadcast_to(kept, (heads, LANES))
-    part[0] = folded
-    part[1] = spread_kept
-    parts[me, 0] = folded
-    parts[me, 1] = spread_kept
-
-    @pl.loop(0, 1)
-    def _(i):
-        for j in range(count - 1):
-            d = dest(j)
-
-            @pl.when(deferred(d))
-            def _():
-                block_copy(d, chunks - 1 - i).start()
-
-    def part_copy(d):
+    part[:pairs] = pack(folded)
+    part[pairs:] = to_row(kept)
+
+    def part_copy(src, dst, to, sent, got):
         return pltpu.make_async_remote_copy(
-            src_ref=part,
-            dst_ref=parts.at[me],
-            send_sem=psend_sem.at[d],
-            recv_sem=precv_sem.at[me],
-            device_id={"sp": d},
+            src_ref=src,
+            dst_ref=dst,
+            send_sem=psend_sem.at[sent],
+            recv_sem=precv_sem.at[got],
+            device_id={"sp": to},
             device_id_type=MESH,
         )
 
-    for j in range(count - 1):
-        part_copy(dest(j)).start()
-
-    @pl.loop(1, chunks)
-    def _(i):
-        for j in range(count - 1):
-            d = dest(j)
-
-            @pl.when(deferred(d))
-            def _():
-                block_copy(d, chunks - 1 - i).start()
-
-    for j in range(count - 1):
+    def send_deferred(start, stop):
+        @pl.loop(start, stop)
+        def _(i):
+            for j in range(count - 1):
+                d = dest(j)
+                ahead = i >= EARLY if j == half - 1 else True
+
+                @pl.when(jnp.logical_and(deferred(d), ahead))
+                def _():
+                    block_copy(d, chunks - 1 - i).start()
+
+    pause = 2 * EARLY if chunks > 2 * EARLY else chunks
+
+    @pl.when(has_outer)
+    def _():
+        send_deferred(EARLY, pause)
+        part_copy(part, outer_part, inward, 0, 0).wait_recv()
+        sums, row = join_sides(
+            part[:pairs], part[pairs:], outer_part[:pairs], outer_part[pairs:], lower
+        )
+        part[:pairs] = sums
+        part[pairs:] = row
+
+    @pl.when(jnp.logical_not(has_outer))
+    def _():
+        send_deferred(0, EARLY)
+
+    @pl.when(is_inner)
+    def _():
+        part_copy(part, other_part, mate, 0, 1).start()
+
+    @pl.when(jnp.logical_not(is_inner))
+    def _():
+        part_copy(part, outer_part, inward, 0, 0).start()
+
+    @pl.when(has_outer)
+    def _():
+        send_deferred(pause, chunks)
+
+    @pl.when(jnp.logical_not(has_outer))
+    def _():
+        send_deferred(EARLY, chunks)
+
+    @pl.when(is_inner)
+    def _():
+        part_copy(part, other_part, mate, 0, 1).wait_recv()
+        sums, row = join_sides(
+            part[:pairs],
+            part[pairs:],
+            other_part[:pairs],
+            other_part[pairs:],
+            jnp.logical_not(lower),
+        )
+        whole[:pairs] = sums
+        whole[pairs:] = row
+
+    @pl.when(jnp.logical_not(is_inner))
+    def _():
+        part_copy(whole, inner_whole, outward, 1, 2).wait_recv()
+        whole[...] = inner_whole[...]
+
+    packed = whole[:pairs]
+    turned = pltpu.roll(packed, HD, axis=1)
+    low_half = lax.broadcasted_iota(jnp.int32, (1, LANES), 1) < HD
+
+    def head_at(h, side):
+        source = packed if h // group % 2 == side else turned
+        at = h // group // 2 * group + h % group
+        return source[at : at + 1]
+
+    for m in range(pairs):
+        piece = jnp.where(low_half, head_at(2 * m, 0), head_at(2 * m + 1, 1))
+        read_ref[:, m * LANES : (m + 1) * LANES] = piece.astype(read_ref.dtype)
+
+    @pl.when(has_outer)
+    def _():
+        out = part_copy(whole, inner_whole, outward, 1, 2)
+        out.start()
+        out.wait_send()
+
+    part_copy(part, other_part, mate, 0, 1).wait_send()
+    for j in range(count - 2, -1, -1):
         d = dest(j)
-        pltpu.make_async_remote_copy(
-            src_ref=part,
-            dst_ref=parts.at[d],
-            send_sem=psend_sem.at[d],
-            recv_sem=precv_sem.at[d],
-            device_id={"sp": d},
-            device_id_type=MESH,
-        ).wait()
-    left = jnp.zeros((heads, LANES), jnp.float32)
-    out = jnp.zeros((heads, LANES), jnp.float32)
-    for z in range(count - 1, -1, -1):
-        out = out + jnp.exp(left) * parts[z, 0]
-        left = left + parts[z, 1]
-    turned = pltpu.roll(out, HD, axis=1)
-    low_half = lax.broadcasted_iota(jnp.int32, (1, LANES), 1) < HD
-    for m in range(heads // 2):
-        first, second = 2 * m, 2 * m + 1
-        from_first = out if (first // group) % 2 == 0 else turned
-        from_second = out if (second // group) % 2 == 1 else turned
-        piece = jnp.where(
-            low_half, from_first[first : first + 1], from_second[second : second + 1]
-        )
-        read_ref[:, m * LANES : (m + 1) * LANES] = piece.astype(read_ref.dtype)
-    for j in range(count - 1):
-        d = dest(j)
-        pltpu.make_async_remote_copy(
+        copy = pltpu.make_async_remote_copy(
             src_ref=proj.at[d],
             dst_ref=recv.at[pl.ds(pl.multiple_of(d * rows, CHUNK), rows), :],
             send_sem=send_sem.at[d],
             recv_sem=recv_sem.at[d],
             device_id={"sp": d},
             device_id_type=MESH,
-        ).wait()
-
-
-def place_kernel(count, got, read, cache, read_out, sems):
-    rows = got.shape[0] // count
+        )
+        copy.wait()
+
+
+def place_kernel(got, read, cache, read_out, sems):
+    rows = got.shape[0] // PLACES
     copies = []
-    for k in range(count):
+    for k in range(PLACES):
         at = pl.ds(k * rows, rows)
         copies.append(pltpu.make_async_copy(got.at[at, :], cache.at[at, :], sems.at[k]))
-    copies.append(pltpu.make_async_copy(read, read_out, sems.at[count]))
+    copies.append(pltpu.make_async_copy(read, read_out, sems.at[PLACES]))
     for copy in copies:
         copy.start()
     for copy in copies:
@@ -364,10 +539,12 @@
         and count > 2
         and width % LANES == 0
         and rows % CHUNK == 0
-        and rows >= 2 * CHUNK
+        and rows > EARLY * CHUNK
+        and model_width % (SLICES * LANES) == 0
         and features == 2 * KVH * HD
         and 2 * HD == LANES
-        and heads % 2 == 0
+        and heads % KVH == 0
+        and heads <= LANES
     )
     if not fits:
         return local_plain(tokens, kv_weight, queries, score_offset)
@@ -387,14 +564,16 @@
             pltpu.VMEM((count, model_width, width), jnp.bfloat16),
             pltpu.VMEM((count, rows, width), jnp.bfloat16),
             pltpu.VMEM((heads, KVH * HD), jnp.bfloat16),
-            pltpu.VMEM((2, heads, LANES), jnp.float32),
-            pltpu.VMEM((count, 2, heads, LANES), jnp.float32),
+            *[pltpu.VMEM((heads // 2 + 1, LANES), jnp.float32)] * 5,
             pltpu.SemaphoreType.DMA((rows // CHUNK,)),
             pltpu.SemaphoreType.DMA((count,)),
+            pltpu.SemaphoreType.DMA((SLICES,)),
             pltpu.SemaphoreType.DMA((count,)),
             pltpu.SemaphoreType.DMA((count,)),
-            pltpu.SemaphoreType.DMA((count,)),
-            pltpu.SemaphoreType.DMA((count,)),
+            pltpu.SemaphoreType.DMA((2,)),
+            pltpu.SemaphoreType.DMA((3,)),
+            pltpu.SemaphoreType.REGULAR,
+            pltpu.SemaphoreType.REGULAR,
         ],
         compiler_params=pltpu.CompilerParams(
             collective_id=0, has_side_effects=True, vmem_limit_bytes=VMEM_LIMIT
@@ -406,14 +585,14 @@
         score_offset.reshape(1, heads),
     )
     cache, read = pl.pallas_call(
-        functools.partial(place_kernel, count),
+        place_kernel,
         out_shape=(
             jax.ShapeDtypeStruct((length, width), jnp.bfloat16),
             jax.ShapeDtypeStruct((1, heads * HD), jnp.bfloat16),
         ),
         in_specs=[vmem, vmem],
         out_specs=(hbm, hbm),
-        scratch_shapes=[pltpu.SemaphoreType.DMA((count + 1,))],
+        scratch_shapes=[pltpu.SemaphoreType.DMA((PLACES + 1,))],
         compiler_params=pltpu.CompilerParams(vmem_limit_bytes=8 * 2**20),
     )(got, read)
     return cache.reshape(1, 1, length, width), read

time: 101 us -> 98.4 us (0.974)
  Pallas kernels: 99.7 us -> 97.5 us
    pallas_call x1, Pallas kernels: 97.7 us -> 95.5 us  [local(): pl.pallas_call(functools.partial(exchange_kernel, count), out_shape=(pltp...]
where the time goes in v1:
time: 98.4 us; the launch traced here: 98.1 us
  Pallas kernels  97.5 us (99%)
    pallas_call x1, Pallas kernels, local(): pl.pallas_call(functools.partial(exchange_kernel, count), out_shape=(pltp...  95.5 us
    pallas_call x1, Pallas kernels, local(): pl.pallas_call(place_kernel, out_shape=(jax.ShapeDtypeStruct((length, wid...  2.05 us

profile of v1, /device:TPU:9, one launch (start us, length us, event | category | flops | bytes accessed | tf_op | source)
XLA Modules:
  0.0 98.1 jit_solution(13629327900482765458)
XLA Ops:
  0.6 95.5 %shard_map.59 = (bf16[8192,256]{1,0:T(8,128)(2,1)S(1)}, bf16[1,1536]{1,0:T(2,128)(2,1)S(1)}) custom-call(bf16[2048,2048]{1,0:T(8,128)(2,1)} %bitcast.3, bf16[2048,1024]{1,0:T(8,128)(2,1)} %w_hbm.1, bf16[1,1536]{1,0:T(2,128)(2,1)} %q_ref.1, f32[1,24]{1,0:T(1,128)} %bitcast.4), custom_call_target="tpu_custom_call" | custom-call | tf_op jit(solution)/shard_map/pallas_call | solution.py:554
  96.1 2.1 %shard_map.60 = (bf16[8192,256]{1,0:T(8,128)(2,1)}, bf16[1,1536]{1,0:T(2,128)(2,1)}) custom-call(bf16[8192,256]{1,0:T(8,128)(2,1)S(1)} %get-tuple-element.6.got, bf16[1,1536]{1,0:T(2,128)(2,1)S(1)} %get-tuple-element.7.read), custom_call_target="tpu_custom_call" | custom-call | tf_op jit(solution)/shard_map/pallas_call | solution.py:587

commit v2 on v1

--- a/solution.py
+++ b/solution.py
@@ -81,40 +81,46 @@
 
 
 CHUNK = 128
+FIRST = 64
 EARLY = 4
 SLICES = 4
-PLACES = 4
-VMEM_LIMIT = 56 * 2**20
+LATE = 12
+VMEM_LIMIT = 51 * 2**20
 LANES = 128
 MESH = pl.DeviceIdType.MESH
+
+
+def is_late(count):
+    me = lax.axis_index("sp")
+    in_middle = jnp.logical_or(me == count // 2 - 1, me == count // 2)
+    return jnp.logical_and(in_middle, lax.rem(lax.axis_index("tp"), 2) == 1)
 
 
 def exchange_kernel(
     count,
     tok_hbm,
     w_hbm,
+    q_hbm,
+    off_hbm,
+    recv,
+    read_ref,
+    proj,
+    tok,
+    wts,
     q_ref,
     off_ref,
-    recv,
-    read_ref,
-    tok,
-    wts,
-    proj,
     qbig,
     part,
     whole,
     outer_part,
     other_part,
     inner_whole,
-    tok_sem,
-    w_sem,
-    slice_sem,
+    load_sem,
     send_sem,
     recv_sem,
     psend_sem,
     precv_sem,
     ready,
-    everyone,
 ):
     me = lax.axis_index("sp")
     rows = tok.shape[0]
@@ -148,59 +154,77 @@
         return pl.ds(pl.multiple_of(c * CHUNK, CHUNK), CHUNK)
 
     def tok_copy(c):
-        return pltpu.make_async_copy(tok_hbm.at[span(c), :], tok.at[span(c), :], tok_sem.at[c])
+        sem = load_sem.at[lax.rem(c, EARLY)]
+        return pltpu.make_async_copy(tok_hbm.at[span(c), :], tok.at[span(c), :], sem)
 
     def w_copy(d):
         at = pl.ds(pl.multiple_of(d * width, width), width)
-        return pltpu.make_async_copy(w_hbm.at[:, at], wts.at[d], w_sem.at[d])
+        return pltpu.make_async_copy(w_hbm.at[:, at], wts.at[d], load_sem.at[EARLY + 2])
 
     def slice_copy(k):
         at = pl.ds(pl.multiple_of(mate * width, width), width)
         deep = pl.ds(k * depth, depth)
         return pltpu.make_async_copy(
-            w_hbm.at[deep, at], wts.at[mate, deep, :], slice_sem.at[k]
-        )
-
-    def block_copy(d, c):
-        there = pl.ds(pl.multiple_of(me * rows + c * CHUNK, CHUNK), CHUNK)
+            w_hbm.at[deep, at], wts.at[mate, deep, :], load_sem.at[EARLY + k]
+        )
+
+    def rows_copy(d, start, size):
+        here = pl.ds(pl.multiple_of(start, FIRST), size)
+        there = pl.ds(pl.multiple_of(me * rows + start, FIRST), size)
         return pltpu.make_async_remote_copy(
-            src_ref=proj.at[d, span(c), :],
+            src_ref=proj.at[d, here, :],
             dst_ref=recv.at[there, :],
-            send_sem=send_sem.at[d],
-            recv_sem=recv_sem.at[me],
+            send_sem=send_sem,
+            recv_sem=recv_sem,
             device_id={"sp": d},
             device_id_type=MESH,
         )
 
+    def block_copy(d, c):
+        return rows_copy(d, c * CHUNK, CHUNK)
+
+    def top_copy(start, size, sem):
+        at = pl.ds(start, size)
+        return pltpu.make_async_copy(tok_hbm.at[at, :], tok.at[at, :], load_sem.at[sem])
+
     barrier = pltpu.get_barrier_semaphore()
 
     @pl.when(is_inner)
     def _():
         pl.semaphore_signal(barrier, inc=1, device_id={"sp": mate}, device_id_type=MESH)
 
-    tok_copy(chunks - 1).start()
+    first_at, rest_at = rows - FIRST, rows - CHUNK
+    first_copy = top_copy(first_at, FIRST, EARLY + SLICES)
+    rest_copy = top_copy(rest_at, CHUNK - FIRST, (chunks - 1) % EARLY)
+    first_copy.start()
     for k in range(SLICES):
         slice_copy(k).start()
-
-    first = jnp.zeros((CHUNK, width), jnp.float32)
-    tok_copy(chunks - 1).wait()
+    rest_copy.start()
+    tok_copy(chunks - 2).start()
+
+    first = jnp.zeros((FIRST, width), jnp.float32)
+    first_copy.wait()
     for k in range(SLICES):
         slice_copy(k).wait()
         if k == 0:
-            tok_copy(chunks - 2).start()
-            w_copy(dest(0)).start()
+            for early_chunk in range(2, EARLY):
+                tok_copy(chunks - 1 - early_chunk).start()
         deep = pl.ds(k * depth, depth)
         first = first + jnp.dot(
-            tok[span(chunks - 1), deep], wts[mate, deep, :], preferred_element_type=jnp.float32
-        )
-    proj[mate, span(chunks - 1), :] = first.astype(jnp.bfloat16)
-    for k in range(2, EARLY):
-        tok_copy(chunks - 1 - k).start()
-    for j in range(1, count):
+            tok[pl.ds(first_at, FIRST), deep], wts[mate, deep, :], preferred_element_type=jnp.float32
+        )
+    proj[mate, pl.ds(first_at, FIRST), :] = first.astype(jnp.bfloat16)
+    small_copies = [
+        pltpu.make_async_copy(q_hbm, q_ref, load_sem.at[EARLY]),
+        pltpu.make_async_copy(off_hbm, off_ref, load_sem.at[EARLY + 1]),
+    ]
+    for j in range(count):
         if j != half - 1:
             w_copy(dest(j)).start()
+    for copy in small_copies:
+        copy.start()
     pl.semaphore_wait(barrier, 1)
-    block_copy(mate, chunks - 1).start()
+    rows_copy(mate, first_at, FIRST).start()
 
     for d in range(count):
         same = (d < half) == lower
@@ -213,6 +237,11 @@
     def _():
         for d in (half - 1, half):
             pl.semaphore_signal(ready, inc=1, device_id={"sp": d}, device_id_type=MESH)
+
+    rest_copy.wait()
+    proj[mate, pl.ds(rest_at, CHUNK - FIRST), :] = jnp.dot(
+        tok[pl.ds(rest_at, CHUNK - FIRST), :], wts[mate], preferred_element_type=jnp.float32
+    ).astype(jnp.bfloat16)
 
     def early(k, carry):
         c = chunks - 1 - k
@@ -221,6 +250,10 @@
             tok[span(c), :], wts[mate], preferred_element_type=jnp.float32
         ).astype(jnp.bfloat16)
 
+        @pl.when(k == 1)
+        def _():
+            rows_copy(mate, rest_at, CHUNK - FIRST).start()
+
         @pl.when(k > 1)
         def _():
             block_copy(mate, c + 1).start()
@@ -228,6 +261,8 @@
         return carry
 
     lax.fori_loop(1, EARLY, early, 0)
+    for copy in small_copies:
+        copy.wait()
 
     q_rows = []
     for h in range(heads):
@@ -279,11 +314,14 @@
 
         @pl.when(jnp.logical_and(is_inner, jnp.logical_and(same, d != me)))
         def _():
-            pl.semaphore_signal(everyone, inc=1, device_id={"sp": d}, device_id_type=MESH)
+            pl.semaphore_signal(ready, inc=1, device_id={"sp": d}, device_id_type=MESH)
 
     @pl.when(jnp.logical_not(is_inner))
     def _():
-        pl.semaphore_wait(everyone, 1)
+        pl.semaphore_wait(ready, 1)
+
+    others = pl.ds(0, count - 1)
+    pltpu.make_async_copy(wts.at[others], wts.at[others], load_sem.at[EARLY + 2]).wait()
 
     def deferred(d):
         crosses = (d < half) != lower
@@ -316,10 +354,6 @@
                     ).astype(jnp.bfloat16)
 
             else:
-
-                @pl.when(i == 0)
-                def _():
-                    w_copy(d).wait()
 
                 block = jnp.dot(
                     tok[at, :], wts[d], preferred_element_type=jnp.float32
@@ -431,7 +465,9 @@
                 def _():
                     block_copy(d, chunks - 1 - i).start()
 
-    pause = 2 * EARLY if chunks > 2 * EARLY else chunks
+    late = is_late(count)
+    stop = jnp.where(late, chunks - LATE, chunks)
+    pause = jnp.minimum(2 * EARLY, stop)
 
     @pl.when(has_outer)
     def _():
@@ -457,7 +493,7 @@
 
     @pl.when(has_outer)
     def _():
-        send_deferred(pause, chunks)
+        send_deferred(pause, stop)
 
     @pl.when(jnp.logical_not(has_outer))
     def _():
@@ -478,7 +514,7 @@
 
     @pl.when(jnp.logical_not(is_inner))
     def _():
-        part_copy(whole, inner_whole, outward, 1, 2).wait_recv()
+        part_copy(whole, inner_whole, outward, 1, 1).wait_recv()
         whole[...] = inner_whole[...]
 
     packed = whole[:pairs]
@@ -496,34 +532,97 @@
 
     @pl.when(has_outer)
     def _():
-        out = part_copy(whole, inner_whole, outward, 1, 2)
+        out = part_copy(whole, inner_whole, outward, 1, 1)
         out.start()
         out.wait_send()
 
     part_copy(part, other_part, mate, 0, 1).wait_send()
-    for j in range(count - 2, -1, -1):
-        d = dest(j)
+    def finish_blocks(size):
+        foreign = pl.ds(0, size)
+        blocks = pltpu.make_async_remote_copy(
+            src_ref=recv.at[foreign, :],
+            dst_ref=recv.at[foreign, :],
+            send_sem=send_sem,
+            recv_sem=recv_sem,
+            device_id={"sp": mate},
+            device_id_type=MESH,
+        )
+        blocks.wait_send()
+        blocks.wait_recv()
+
+    @pl.when(late)
+    def _():
+        finish_blocks((count - 1) * rows - LATE * CHUNK)
+
+    @pl.when(jnp.logical_not(late))
+    def _():
+        finish_blocks((count - 1) * rows)
+
+
+def second_kernel(count, proj, _, rest, send_sem, recv_sem):
+    me = lax.axis_index("sp")
+    mate = jnp.where(me < count // 2, count // 2, count // 2 - 1)
+
+    @pl.when(is_late(count))
+    def _():
+        barrier = pltpu.get_barrier_semaphore()
+        pl.semaphore_signal(barrier, inc=1, device_id={"sp": mate}, device_id_type=MESH)
+        pl.semaphore_wait(barrier, 1)
         copy = pltpu.make_async_remote_copy(
-            src_ref=proj.at[d],
-            dst_ref=recv.at[pl.ds(pl.multiple_of(d * rows, CHUNK), rows), :],
-            send_sem=send_sem.at[d],
-            recv_sem=recv_sem.at[d],
-            device_id={"sp": d},
+            src_ref=proj.at[mate, pl.ds(0, LATE * CHUNK), :],
+            dst_ref=rest,
+            send_sem=send_sem,
+            recv_sem=recv_sem,
+            device_id={"sp": mate},
             device_id_type=MESH,
         )
+        copy.start()
         copy.wait()
 
 
-def place_kernel(got, read, cache, read_out, sems):
-    rows = got.shape[0] // PLACES
-    copies = []
-    for k in range(PLACES):
-        at = pl.ds(k * rows, rows)
-        copies.append(pltpu.make_async_copy(got.at[at, :], cache.at[at, :], sems.at[k]))
-    copies.append(pltpu.make_async_copy(read, read_out, sems.at[PLACES]))
-    for copy in copies:
+def place_kernel(count, got, read, cache, read_out, sem, read_sem):
+    rows = got.shape[0] // count
+    me = lax.axis_index("sp")
+    mate = jnp.where(me < count // 2, count // 2, count // 2 - 1)
+    late = is_late(count)
+
+    def copy(start, size):
+        at = pl.ds(pl.multiple_of(start, CHUNK), size)
+        return pltpu.make_async_copy(got.at[at, :], cache.at[at, :], sem)
+
+    read_copy = pltpu.make_async_copy(read, read_out, read_sem)
+    for d in range(count):
+
+        @pl.when(jnp.logical_and(late, d == mate))
+        def _():
+            copy(d * rows + LATE * CHUNK, rows - LATE * CHUNK).start()
+
+        @pl.when(jnp.logical_not(jnp.logical_and(late, d == mate)))
+        def _():
+            copy(d * rows, rows).start()
+
+    read_copy.start()
+    read_copy.wait()
+
+    @pl.when(late)
+    def _():
+        copy(0, count * rows - LATE * CHUNK).wait()
+
+    @pl.when(jnp.logical_not(late))
+    def _():
+        copy(0, count * rows).wait()
+
+
+def complete_kernel(count, rest, _, cache, sem):
+    rows = cache.shape[0] // count
+    me = lax.axis_index("sp")
+    mate = jnp.where(me < count // 2, count // 2, count // 2 - 1)
+
+    @pl.when(is_late(count))
+    def _():
+        at = pl.ds(pl.multiple_of(mate * rows, CHUNK), LATE * CHUNK)
+        copy = pltpu.make_async_copy(rest, cache.at[at, :], sem)
         copy.start()
-    for copy in copies:
         copy.wait()
 
 
@@ -539,11 +638,12 @@
         and count > 2
         and width % LANES == 0
         and rows % CHUNK == 0
-        and rows > EARLY * CHUNK
+        and rows >= (EARLY + LATE) * CHUNK
         and model_width % (SLICES * LANES) == 0
         and features == 2 * KVH * HD
         and 2 * HD == LANES
         and heads % KVH == 0
+        and rows // CHUNK % EARLY == 0
         and heads <= LANES
     )
     if not fits:
@@ -551,28 +651,27 @@
     length = rows * count
     vmem = pl.BlockSpec(memory_space=pltpu.VMEM)
     hbm = pl.BlockSpec(memory_space=pltpu.HBM)
-    got, read = pl.pallas_call(
+    got, read, proj = pl.pallas_call(
         functools.partial(exchange_kernel, count),
         out_shape=(
             pltpu.VMEM((length, width), jnp.bfloat16),
             pltpu.VMEM((1, heads * HD), jnp.bfloat16),
+            pltpu.VMEM((count, rows, width), jnp.bfloat16),
         ),
-        in_specs=[hbm, hbm, vmem, vmem],
-        out_specs=(vmem, vmem),
+        in_specs=[hbm, hbm, hbm, hbm],
+        out_specs=(vmem, vmem, vmem),
         scratch_shapes=[
             pltpu.VMEM((rows, model_width), jnp.bfloat16),
             pltpu.VMEM((count, model_width, width), jnp.bfloat16),
-            pltpu.VMEM((count, rows, width), jnp.bfloat16),
+            pltpu.VMEM((1, heads * HD), jnp.bfloat16),
+            pltpu.VMEM((1, heads), jnp.float32),
             pltpu.VMEM((heads, KVH * HD), jnp.bfloat16),
             *[pltpu.VMEM((heads // 2 + 1, LANES), jnp.float32)] * 5,
-            pltpu.SemaphoreType.DMA((rows // CHUNK,)),
-            pltpu.SemaphoreType.DMA((count,)),
-            pltpu.SemaphoreType.DMA((SLICES,)),
-            pltpu.SemaphoreType.DMA((count,)),
-            pltpu.SemaphoreType.DMA((count,)),
+            pltpu.SemaphoreType.DMA((EARLY + SLICES + 1,)),
+            pltpu.SemaphoreType.DMA,
+            pltpu.SemaphoreType.DMA,
             pltpu.SemaphoreType.DMA((2,)),
-            pltpu.SemaphoreType.DMA((3,)),
-            pltpu.SemaphoreType.REGULAR,
+            pltpu.SemaphoreType.DMA((2,)),
             pltpu.SemaphoreType.REGULAR,
         ],
         compiler_params=pltpu.CompilerParams(
@@ -585,16 +684,35 @@
         score_offset.reshape(1, heads),
     )
     cache, read = pl.pallas_call(
-        place_kernel,
+        functools.partial(place_kernel, count),
         out_shape=(
             jax.ShapeDtypeStruct((length, width), jnp.bfloat16),
             jax.ShapeDtypeStruct((1, heads * HD), jnp.bfloat16),
         ),
         in_specs=[vmem, vmem],
         out_specs=(hbm, hbm),
-        scratch_shapes=[pltpu.SemaphoreType.DMA((PLACES + 1,))],
-        compiler_params=pltpu.CompilerParams(vmem_limit_bytes=8 * 2**20),
+        scratch_shapes=[pltpu.SemaphoreType.DMA, pltpu.SemaphoreType.DMA],
+        compiler_params=pltpu.CompilerParams(vmem_limit_bytes=24 * 2**20),
     )(got, read)
+    rest = pl.pallas_call(
+        functools.partial(second_kernel, count),
+        out_shape=pltpu.VMEM((LATE * CHUNK, width), jnp.bfloat16),
+        in_specs=[vmem, hbm],
+        out_specs=vmem,
+        scratch_shapes=[pltpu.SemaphoreType.DMA, pltpu.SemaphoreType.DMA],
+        compiler_params=pltpu.CompilerParams(
+            collective_id=1, has_side_effects=True, vmem_limit_bytes=24 * 2**20
+        ),
+    )(proj, read)
+    cache = pl.pallas_call(
+        functools.partial(complete_kernel, count),
+        out_shape=jax.ShapeDtypeStruct((length, width), jnp.bfloat16),
+        in_specs=[vmem, hbm],
+        out_specs=hbm,
+        scratch_shapes=[pltpu.SemaphoreType.DMA],
+        input_output_aliases={1: 0},
+        compiler_params=pltpu.CompilerParams(vmem_limit_bytes=24 * 2**20),
+    )(rest, cache)
     return cache.reshape(1, 1, length, width), read
 
 

time: 98.4 us -> 96.1 us (0.977)
  Pallas kernels: 97.5 us -> 94.5 us
    pallas_call x1, Pallas kernels: 95.5 us -> 78.1 us  [local(): pl.pallas_call(functools.partial(exchange_kernel, count), out_shape=(pltp...]
    pallas_call x1 -> x3, Pallas kernels: 2.05 us -> 16.4 us  [the longest x1 13.7 us: local(): pl.pallas_call(functools.partial(second_kernel, count), out_shape=pltpu.V...]
where the time goes in v2:
time: 96.1 us; the launch traced here: 95.9 us
  Pallas kernels  94.5 us (98%)
    pallas_call x1, Pallas kernels, local(): pl.pallas_call(functools.partial(exchange_kernel, count), out_shape=(pltp...  78.1 us
    pallas_call x1, Pallas kernels, local(): pl.pallas_call(functools.partial(second_kernel, count), out_shape=pltpu.V...  13.7 us

profile of v2, /device:TPU:9, one launch (start us, length us, event | category | flops | bytes accessed | tf_op | source)
XLA Modules:
  0.0 95.9 jit_solution(16013597378367741426)
XLA Ops:
  0.6 78.1 %shard_map.59 = (bf16[8192,256]{1,0:T(8,128)(2,1)S(1)}, bf16[1,1536]{1,0:T(2,128)(2,1)S(1)}, bf16[4,2048,256]{2,1,0:T(8,128)(2,1)S(1)}) custom-call(bf16[2048,2048]{1,0:T(8,128)(2,1)} %bitcast.3, bf16[2048,1024]{1,0:T(8,128)(2,1)} %w_hbm.1, bf16[1,1536]{1,0:T(2,128)(2,1)} %q_hbm.1, f32[1,24]{1,0:T(1,128)} %bitcast.5), custom_call_target="tpu_custom_call" | custom-call | tf_op jit(solution)/shard_map/pallas_call | solution.py:654
  78.8 1.8 %shard_map.60 = (bf16[8192,256]{1,0:T(8,128)(2,1)}, bf16[1,1536]{1,0:T(2,128)(2,1)}) custom-call(bf16[8192,256]{1,0:T(8,128)(2,1)S(1)} %get-tuple-element.8.got, bf16[1,1536]{1,0:T(2,128)(2,1)S(1)} %get-tuple-element.9.read), custom_call_target="tpu_custom_call" | custom-call | tf_op jit(solution)/shard_map/pallas_call | solution.py:686
  80.5 0.0 copy-start
  80.6 0.7 copy-done
  81.2 13.7 %shard_map.61.rest = bf16[1536,256]{1,0:T(8,128)(2,1)S(1)} custom-call(bf16[4,2048,256]{2,1,0:T(8,128)(2,1)S(1)} %get-tuple-element.7.proj, bf16[1,1536]{1,0:T(2,128)(2,1)S(1)} %copy-done), custom_call_target="tpu_custom_call" | custom-call | tf_op jit(solution)/shard_map/pallas_call | solution.py:697
  95.0 0.9 shard_map.62
Async XLA Ops:
  80.5 0.7 copy-start

commit v3 on v2

--- a/solution.py
+++ b/solution.py
@@ -83,7 +83,7 @@
 CHUNK = 128
 FIRST = 64
 EARLY = 4
-SLICES = 4
+SLICES = 2
 LATE = 12
 VMEM_LIMIT = 51 * 2**20
 LANES = 128
@@ -131,6 +131,7 @@
     group = heads // KVH
     half = count // 2
     depth = model_width // SLICES
+    sides = width // LANES
 
     lower = me < half
     inner = jnp.where(lower, half - 1, half)
@@ -161,19 +162,20 @@
         at = pl.ds(pl.multiple_of(d * width, width), width)
         return pltpu.make_async_copy(w_hbm.at[:, at], wts.at[d], load_sem.at[EARLY + 2])
 
-    def slice_copy(k):
-        at = pl.ds(pl.multiple_of(mate * width, width), width)
-        deep = pl.ds(k * depth, depth)
+    def slice_copy(side, k):
+        at = pl.ds(pl.multiple_of(mate * width + side * LANES, LANES), LANES)
         return pltpu.make_async_copy(
-            w_hbm.at[deep, at], wts.at[mate, deep, :], load_sem.at[EARLY + k]
-        )
-
-    def rows_copy(d, start, size):
+            w_hbm.at[pl.ds(k * depth, depth), at],
+            wts.at[mate, pl.ds(k * depth, depth), pl.ds(side * LANES, LANES)],
+            load_sem.at[EARLY + side * SLICES + k],
+        )
+
+    def rows_copy(d, start, size, columns=pl.ds(0, width)):
         here = pl.ds(pl.multiple_of(start, FIRST), size)
         there = pl.ds(pl.multiple_of(me * rows + start, FIRST), size)
         return pltpu.make_async_remote_copy(
-            src_ref=proj.at[d, here, :],
-            dst_ref=recv.at[there, :],
+            src_ref=proj.at[d, here, columns],
+            dst_ref=recv.at[there, columns],
             send_sem=send_sem,
             recv_sem=recv_sem,
             device_id={"sp": d},
@@ -194,37 +196,43 @@
         pl.semaphore_signal(barrier, inc=1, device_id={"sp": mate}, device_id_type=MESH)
 
     first_at, rest_at = rows - FIRST, rows - CHUNK
-    first_copy = top_copy(first_at, FIRST, EARLY + SLICES)
+    first_copy = top_copy(first_at, FIRST, EARLY + sides * SLICES)
     rest_copy = top_copy(rest_at, CHUNK - FIRST, (chunks - 1) % EARLY)
     first_copy.start()
-    for k in range(SLICES):
-        slice_copy(k).start()
+    for side in range(sides):
+        for k in range(SLICES):
+            slice_copy(side, k).start()
     rest_copy.start()
     tok_copy(chunks - 2).start()
 
-    first = jnp.zeros((FIRST, width), jnp.float32)
-    first_copy.wait()
-    for k in range(SLICES):
-        slice_copy(k).wait()
-        if k == 0:
-            for early_chunk in range(2, EARLY):
-                tok_copy(chunks - 1 - early_chunk).start()
-        deep = pl.ds(k * depth, depth)
-        first = first + jnp.dot(
-            tok[pl.ds(first_at, FIRST), deep], wts[mate, deep, :], preferred_element_type=jnp.float32
-        )
-    proj[mate, pl.ds(first_at, FIRST), :] = first.astype(jnp.bfloat16)
     small_copies = [
         pltpu.make_async_copy(q_hbm, q_ref, load_sem.at[EARLY]),
         pltpu.make_async_copy(off_hbm, off_ref, load_sem.at[EARLY + 1]),
     ]
+    first_copy.wait()
+    for side in range(sides):
+        lanes = pl.ds(side * LANES, LANES)
+        first = jnp.zeros((FIRST, LANES), jnp.float32)
+        for k in range(SLICES):
+            slice_copy(side, k).wait()
+            deep = pl.ds(k * depth, depth)
+            first = first + jnp.dot(
+                tok[pl.ds(first_at, FIRST), deep],
+                wts[mate, deep, lanes],
+                preferred_element_type=jnp.float32,
+            )
+        proj[mate, pl.ds(first_at, FIRST), lanes] = first.astype(jnp.bfloat16)
+        if side == 0:
+            for early_chunk in range(2, EARLY):
+                tok_copy(chunks - 1 - early_chunk).start()
+            pl.semaphore_wait(barrier, 1)
+        else:
+            for copy in small_copies if side == 1 else ():
+                copy.start()
+        rows_copy(mate, first_at, FIRST, lanes).start()
     for j in range(count):
         if j != half - 1:
             w_copy(dest(j)).start()
-    for copy in small_copies:
-        copy.start()
-    pl.semaphore_wait(barrier, 1)
-    rows_copy(mate, first_at, FIRST).start()
 
     for d in range(count):
         same = (d < half) == lower
@@ -246,13 +254,14 @@
     def early(k, carry):
         c = chunks - 1 - k
         tok_copy(c).wait()
+
+        @pl.when(k == 1)
+        def _():
+            rows_copy(mate, rest_at, CHUNK - FIRST).start()
+
         proj[mate, span(c), :] = jnp.dot(
             tok[span(c), :], wts[mate], preferred_element_type=jnp.float32
         ).astype(jnp.bfloat16)
-
-        @pl.when(k == 1)
-        def _():
-            rows_copy(mate, rest_at, CHUNK - FIRST).start()
 
         @pl.when(k > 1)
         def _():
@@ -667,7 +676,7 @@
             pltpu.VMEM((1, heads), jnp.float32),
             pltpu.VMEM((heads, KVH * HD), jnp.bfloat16),
             *[pltpu.VMEM((heads // 2 + 1, LANES), jnp.float32)] * 5,
-            pltpu.SemaphoreType.DMA((EARLY + SLICES + 1,)),
+            pltpu.SemaphoreType.DMA((EARLY + width // LANES * SLICES + 1,)),
             pltpu.SemaphoreType.DMA,
             pltpu.SemaphoreType.DMA,
             pltpu.SemaphoreType.DMA((2,)),

time: 96.1 us -> 95.7 us (level)
  no operation moved by 1% of the time
where the time goes in v3:
time: 95.7 us; the launch traced here: 95.5 us
  Pallas kernels  94.1 us (98%)
    pallas_call x1, Pallas kernels, local(): pl.pallas_call(functools.partial(exchange_kernel, count), out_shape=(pltp...  77.7 us
    pallas_call x1, Pallas kernels, local(): pl.pallas_call(functools.partial(second_kernel, count), out_shape=pltpu.V...  13.8 us

profile of v3, /device:TPU:9, one launch (start us, length us, event | category | flops | bytes accessed | tf_op | source)
XLA Modules:
  0.0 95.5 jit_solution(13473663905542485250)
XLA Ops:
  0.6 77.7 %shard_map.59 = (bf16[8192,256]{1,0:T(8,128)(2,1)S(1)}, bf16[1,1536]{1,0:T(2,128)(2,1)S(1)}, bf16[4,2048,256]{2,1,0:T(8,128)(2,1)S(1)}) custom-call(bf16[2048,2048]{1,0:T(8,128)(2,1)} %bitcast.3, bf16[2048,1024]{1,0:T(8,128)(2,1)} %w_hbm.1, bf16[1,1536]{1,0:T(2,128)(2,1)} %q_hbm.1, f32[1,24]{1,0:T(1,128)} %bitcast.5), custom_call_target="tpu_custom_call" | custom-call | tf_op jit(solution)/shard_map/pallas_call | solution.py:663
  78.3 1.8 %shard_map.60 = (bf16[8192,256]{1,0:T(8,128)(2,1)}, bf16[1,1536]{1,0:T(2,128)(2,1)}) custom-call(bf16[8192,256]{1,0:T(8,128)(2,1)S(1)} %get-tuple-element.8.got, bf16[1,1536]{1,0:T(2,128)(2,1)S(1)} %get-tuple-element.9.read), custom_call_target="tpu_custom_call" | custom-call | tf_op jit(solution)/shard_map/pallas_call | solution.py:695
  80.1 0.0 copy-start
  80.1 0.7 copy-done
  80.8 13.8 %shard_map.61.rest = bf16[1536,256]{1,0:T(8,128)(2,1)S(1)} custom-call(bf16[4,2048,256]{2,1,0:T(8,128)(2,1)S(1)} %get-tuple-element.7.proj, bf16[1,1536]{1,0:T(2,128)(2,1)S(1)} %copy-done), custom_call_target="tpu_custom_call" | custom-call | tf_op jit(solution)/shard_map/pallas_call | solution.py:706
  94.6 0.9 shard_map.62
Async XLA Ops:
  80.1 0.7 copy-start
